TPU v7x, 32 devices: a whole 2x2x4 slice. The times are simulated.
32 devices in a mesh: sp: 4 (over z), fs: 4 (over y, x), tp: 2 (over core).
Axes of the slice: x: 2, y: 2, z: 4, core: 2. Of those that a mesh axis runs over, the one named last changes fastest.
Arguments:
- tokens: bfloat16 [4, 3072, 2048], P('fs', 'sp', 'tp'), may hold values from -6 to 6
- in_gain: float32 [2048], replicated, may hold values from 0.1 to 1.9
- ret_query: bfloat16 [2048, 768], P(None, 'tp'), may hold values from -0.125 to 0.125
- ret_key: bfloat16 [2048, 768], P(None, 'tp'), may hold values from -0.125 to 0.125
- ret_value: bfloat16 [2048, 768], P(None, 'tp'), may hold values from -0.125 to 0.125
- att_query: bfloat16 [2048, 768], P(None, 'tp'), may hold values from -8 to 8
- att_key: bfloat16 [2048, 256], P(None, 'tp'), may hold values from -8 to 8
- att_value: bfloat16 [2048, 256], P(None, 'tp'), may hold values from -0.125 to 0.125
- log_decay: float32 [4, 12, 3072], P('fs', 'tp', 'sp'), may hold values from -1.5 to 0
- ret_gain: float32 [768], P('tp'), may hold values from 0.1 to 1.9
- sink_logit: float32 [12], P('tp'), may hold values from 1 to 5
- retentive_exit_matrix: bfloat16 [768, 2048], P('tp'), may hold values from -0.15625 to 0.15625
- out_att: bfloat16 [768, 2048], P('tp'), may hold values from -0.875 to 0.875
Outputs:
- mixed: bfloat16 [4, 3072, 2048], P('fs', ('sp', 'tp'))
All inputs are finite; a program needn't handle non-finite values.
Results may differ from a plain program's by a relative error of at most 0.0085.
Values may be sent and summed in bfloat16 or wider, within the bound.
A program may use at most 128 MiB of HBM per device.

v0:
```python
import jax
import jax.numpy as jnp
from jax import lax
from jax.sharding import PartitionSpec as P

HEAD_DIM = 64
WINDOW = 128


EPS = 1e-06


def prefix_2(value, axis, join, neutral):
    place = lax.axis_index(axis)
    gathered = jax.tree.map(
        lambda a, kind: lax.all_gather(a.astype(kind), axis), value, (jnp.bfloat16, jnp.bfloat16)
    )
    state = jax.tree.map(lambda a, e: jnp.zeros_like(a) + jnp.asarray(e, a.dtype), value, neutral)

    def one(turn, state):
        return join(
            state,
            jax.tree.map(
                lambda a, own: lax.dynamic_index_in_dim(a, turn, 0, False).astype(own.dtype),
                gathered,
                value,
            ),
        )

    return lax.fori_loop(0, place, one, state)


def passed_along(value, axis, by):
    peers = lax.axis_size(axis)
    pairs = [(i, i + by) for i in range(peers) if 0 <= i + by < peers]
    return lax.ppermute(value, axis, pairs)


def attend_window(query_rows, key_ext, value_ext, first_position, sinks):
    length = query_rows.shape[0]
    blocks = length // WINDOW
    heads_kv = key_ext.shape[1] // HEAD_DIM
    heads = query_rows.shape[1] // HEAD_DIM
    group = heads // heads_kv
    shaped_q = query_rows.reshape(blocks, WINDOW, heads_kv, group, HEAD_DIM)
    key_block_list = key_ext.reshape(blocks + 1, WINDOW, heads_kv, HEAD_DIM)
    value_blocks = value_ext.reshape(blocks + 1, WINDOW, heads_kv, HEAD_DIM)
    key_band = jnp.concatenate([key_block_list[:-1], key_block_list[1:]], axis=1)
    value_band = jnp.concatenate([value_blocks[:-1], value_blocks[1:]], axis=1)
    scores = jnp.einsum(
        "nqhgd,nkhd->hgnqk", shaped_q, key_band, preferred_element_type=jnp.float32
    ) * HEAD_DIM ** (-0.5)
    distance = WINDOW + jnp.arange(WINDOW)[:, None] - jnp.arange(2 * WINDOW)[None, :]
    key_position = (
        first_position
        - WINDOW
        + jnp.arange(blocks)[:, None] * WINDOW
        + jnp.arange(2 * WINDOW)[None, :]
    )
    allowed = ((distance >= 0) & (distance < WINDOW))[None] & (key_position >= 0)[:, None, :]
    scores = jnp.where(allowed, scores, -jnp.inf)
    sink_part = sinks.reshape(heads_kv, group, 1, 1, 1)
    greatest_level = jnp.maximum(jnp.max(scores, axis=-1, keepdims=True), sink_part)
    raised = jnp.exp(scores - greatest_level)
    totals = jnp.sum(raised, axis=-1, keepdims=True) + jnp.exp(sink_part - greatest_level)
    weights = (raised / totals).astype(jnp.bfloat16)
    outputs = jnp.einsum(
        "hgnqk,nkhd->nqhgd", weights, value_band, preferred_element_type=jnp.float32
    )
    return outputs.reshape(length, heads * HEAD_DIM).astype(jnp.bfloat16)


def shards(
    tokens,
    in_gain,
    ret_query,
    ret_key,
    ret_value,
    att_query,
    att_key,
    att_value,
    log_decay,
    ret_gain,
    sink_logit,
    retentive_exit_matrix,
    out_att,
):
    rows_here = tokens.shape[1]
    model_width = in_gain.shape[0]
    projections = (ret_query, ret_key, ret_value, att_query, att_key, att_value)
    wide = lax.all_gather(tokens, "tp", axis=2, tiled=True)[0].astype(jnp.float32)
    scaled = (wide * in_gain).astype(jnp.bfloat16)
    sums = tuple(
        (jnp.dot(scaled, weight, preferred_element_type=jnp.float32) for weight in projections)
    )
    sums, squares = (sums, jnp.sum(wide * wide, axis=1, keepdims=True))
    inverse = lax.rsqrt(squares / model_width + EPS)
    ret_q, ret_k, ret_v, att_q, att_k, att_v = [
        (total * inverse).astype(jnp.bfloat16) for total in sums
    ]
    rates = log_decay[0]
    heads = rates.shape[0]
    fading_multiplier = HEAD_DIM ** (-0.5)
    cumulative = jnp.cumsum(rates, axis=1)
    later = jnp.arange(rows_here)[:, None] >= jnp.arange(rows_here)[None, :]
    decay = jnp.exp(
        jnp.where(later[None], cumulative[:, :, None] - cumulative[:, None, :], -jnp.inf)
    )
    shaped_q = ret_q.reshape(rows_here, heads, HEAD_DIM)
    shaped_k = ret_k.reshape(rows_here, heads, HEAD_DIM)
    shaped_v = ret_v.reshape(rows_here, heads, HEAD_DIM)
    weights = (
        jnp.einsum("thd,shd->hts", shaped_q, shaped_k, preferred_element_type=jnp.float32)
        * fading_multiplier
        * decay
    ).astype(jnp.bfloat16)
    inner = jnp.einsum("hts,shd->thd", weights, shaped_v, preferred_element_type=jnp.float32)
    keyed = (
        shaped_k.astype(jnp.float32)
        * (jnp.exp(cumulative[:, -1:] - cumulative) * fading_multiplier).T[:, :, None]
    )
    own_state = jnp.einsum(
        "shd,she->hde", keyed, shaped_v.astype(jnp.float32), precision=lax.Precision.HIGHEST
    )
    total_rate = jnp.exp(cumulative[:, -1])
    tail_keys = att_k[rows_here - WINDOW :]
    trailing_values = att_v[rows_here - WINDOW :]

    def combine(earlier, later_part):
        return (
            earlier[0] * later_part[0],
            later_part[0][:, None, None] * earlier[1] + later_part[1],
        )

    identity = (jnp.ones_like(total_rate), jnp.zeros_like(own_state))
    prefix = prefix_2((total_rate, own_state), "sp", combine, identity)
    incoming = prefix[1]
    before_keys, before_values = passed_along((tail_keys, trailing_values), "sp", 1)
    carried = jnp.einsum(
        "thd,hde->the", shaped_q.astype(jnp.float32), incoming, precision=lax.Precision.HIGHEST
    )
    retained = inner + carried * jnp.exp(cumulative).T[:, :, None]
    normed = retained * lax.rsqrt(jnp.mean(retained * retained, axis=-1, keepdims=True) + EPS)
    ret_out = (normed.reshape(rows_here, heads * HEAD_DIM) * ret_gain).astype(jnp.bfloat16)
    first_position = lax.axis_index("sp") * rows_here
    key_ext = jnp.concatenate([before_keys, att_k], axis=0)
    value_ext = jnp.concatenate([before_values, att_v], axis=0)
    att_out = attend_window(att_q, key_ext, value_ext, first_position, sink_logit)
    ret_rows, att_rows = (
        lax.all_to_all(ret_out, "tp", split_axis=0, concat_axis=1, tiled=True),
        lax.all_to_all(att_out, "tp", split_axis=0, concat_axis=1, tiled=True),
    )
    summed = jnp.dot(
        ret_rows,
        lax.all_gather(retentive_exit_matrix, "tp", axis=0, tiled=True),
        preferred_element_type=jnp.float32,
    ) + jnp.dot(
        att_rows,
        lax.all_gather(out_att, "tp", axis=0, tiled=True),
        preferred_element_type=jnp.float32,
    )
    return summed.astype(jnp.bfloat16)[None]


def solution(mesh):
    return jax.shard_map(
        shards,
        mesh=mesh,
        in_specs=(
            P("fs", "sp", "tp"),
            P(),
            P(None, "tp"),
            P(None, "tp"),
            P(None, "tp"),
            P(None, "tp"),
            P(None, "tp"),
            P(None, "tp"),
            P("fs", "tp", "sp"),
            P("tp"),
            P("tp"),
            P("tp", None),
            P("tp", None),
        ),
        out_specs=P("fs", ("sp", "tp"), None),
        check_vma=False,
    )
```

profile of v0, /device:TPU:0, one launch (start us, length us, event | category | flops | bytes accessed | tf_op | source)
XLA Modules:
  0.0 120.2 jit_solution(14216685554134731407)
XLA Ops:
  6.6 0.7 all-gather.6.cloned.1.call-update
  7.3 0.7 all-gather.8.cloned.1.call-update
  8.1 0.7 all-gather.10.cloned.1.call-update
  8.8 1.0 iota_compare_fusion
  10.0 1.7 %reduce-window.6 = f32[6,6,128]{2,1,0:T(8,128)S(1)} reduce-window(f32[6,6,128]{2,1,0:T(8,128)S(1)} %reshape.202, f32[]{:T(128)} %constant.17.clone.1), window={size=1x1x128 pad=0_0x0_0x127_0}, to_apply=%region_1.0 | reduce-window | flops 585216 | bytes 36868 | tf_op jit(solution)/shard_map/reduce-window
  12.1 0.6 copy-done.4
  12.9 0.6 exponential_bitcast_fusion
  13.5 0.6 dynamic-slice
  14.8 0.2 dynamic-update-slice
  15.1 13.5 %all-reduce = bf16[24]{0:T(256)(128)(2,1)S(1)} all-reduce(bf16[24]{0:T(256)(128)(2,1)S(1)} %dynamic-update-slice), channel_id=2, replica_groups=mesh['sp'=4,'fs'=4,'tp'=2] {'sp'}, use_global_device_ids=true, to_apply=%add | all-reduce | flops 24 | bytes 96
  28.6 0.3 broadcast_and_fusion
  29.0 2.7 %fusion.1 = f32[768]{0:T(1024)S(1)} fusion(bf16[1,768,2048]{2,1,0:T(8,128)(2,1)} %all-gather.6.cloned.1.call-done), kind=kLoop, calls=%fused_computation.6 | loop fusion | flops 4717824 | bytes 3148800 | tf_op jit(solution)/shard_map/reduce_sum | solution.py:96
  31.8 1.0 fusion.39
  32.8 0.6 slice.50
  33.4 1.9 %collective-permute-start.1 = (bf16[128,128]{1,0:T(8,128)(2,1)}, bf16[128,128]{1,0:T(8,128)(2,1)}, u32[]{:S(2)}, u32[]{:S(2)}) collective-permute-start(bf16[128,128]{1,0:T(8,128)(2,1)} %slice.50), channel_id=1, source_target_pairs={{0,8},{8,16},{16,24},{1,9},{9,17},{17,25},{2,10},{10,18},{18,26},{... | collective-permute-start | bytes 98312 | tf_op jit(solution)/shard_map/ppermute | solution.py:36
  35.3 1.0 fusion.42
  36.3 0.6 slice.49
  36.9 2.8 %collective-permute-start = (bf16[128,128]{1,0:T(8,128)(2,1)}, bf16[128,128]{1,0:T(8,128)(2,1)}, u32[]{:S(2)}, u32[]{:S(2)}) collective-permute-start(bf16[128,128]{1,0:T(8,128)(2,1)} %slice.49), channel_id=1, source_target_pairs={{0,8},{8,16},{16,24},{1,9},{9,17},{17,25},{2,10},{10,18},{18,26},{... | collective-permute-start | bytes 98312 | tf_op jit(solution)/shard_map/ppermute | solution.py:36
  39.7 1.4 %fusion.13 = bf16[768,384]{0,1:T(8,128)(2,1)S(1)} fusion(bf16[2048,384]{1,0:T(8,128)(2,1)S(1)} %copy-done, bf16[1,768,2048]{2,1,0:T(8,128)(2,1)S(1)} %copy-done.1, f32[2048]{0:T(1024)S(1)} %copy-done.10, f32[768]{0:T(1024)S(1)} %add_rsqrt_fusion.1), kind=kOutput, calls=%fused_computation.28 | convolution fusion | flops 1213267968 | bytes 5319680 | tf_op jit(solution)/shard_map/dot_general | solution.py:94
  41.2 1.4 %fusion.11 = bf16[768,384]{0,1:T(8,128)(2,1)S(1)} fusion(bf16[2048,384]{1,0:T(8,128)(2,1)S(1)} %copy-done.7, bf16[1,768,2048]{2,1,0:T(8,128)(2,1)S(1)} %copy-done.1, f32[2048]{0:T(1024)S(1)} %copy-done.10, f32[768]{0:T(1024)S(1)} %add_rsqrt_fusion.1), kind=kOutput, calls=%fused_computation.26 | convolution fusion | flops 1213267968 | bytes 5319680 | tf_op jit(solution)/shard_map/dot_general | solution.py:94
  42.6 0.7 fusion.45
  43.4 14.2 %all-gather.1 = bf16[24,64,64]{2,1,0:T(8,128)(2,1)S(1)} all-gather(bf16[6,64,64]{2,1,0:T(8,128)(2,1)S(1)} %fusion.45), channel_id=3, replica_groups=mesh['sp'=4,'fs'=4,'tp'=2] {'sp'}, dimensions={0}, use_global_device_ids=true | all-gather | bytes 245760 | tf_op jit(solution)/shard_map/all_gather | solution.py:16
  57.6 0.2 while.12
  57.8 4.6 %fusion.12 = bf16[768,384]{0,1:T(8,128)(2,1)} fusion(bf16[2048,384]{1,0:T(8,128)(2,1)} %param.17, bf16[1,768,2048]{2,1,0:T(8,128)(2,1)} %all-gather.6.cloned.1.call-done, f32[2048]{0:T(1024)S(1)} %copy-done.10, f32[768]{0:T(1024)S(1)} %add_rsqrt_fusion.1), kind=kOutput, calls=%fused_computation.27 | convolution fusion | flops 1213267968 | bytes 5319680 | tf_op jit(solution)/shard_map/dot_general | solution.py:94
  62.4 7.6 %fusion.8 = f32[768,6,64]{0,2,1:T(8,128)S(1)} fusion(bf16[768,6,64]{0,2,1:T(8,128)(2,1)} %bitcast.124, bf16[768,6,64]{0,2,1:T(8,128)(2,1)} %bitcast.115, bf16[768,6,64]{0,2,1:T(8,128)(2,1)} %bitcast.122, f32[6,768]{1,0:T(8,128)} %bitcast.118, pred[768,768]{1,0:T(8,128)(4,1)} %iota_compare_fusion), kind=kOutput, calls=%fused_computation.22 | convolution fusion | flops 923664384 | bytes 3557376 | tf_op jit(solution)/shard_map/hts,shd->thd/dot_general | solution.py:117
  70.0 1.9 %multiply_reduce_fusion = (f32[768,6]{0,1:T(8,128)S(1)}, f32[768,6,64]{0,2,1:T(8,128)S(1)}) fusion(f32[768,6,64]{0,2,1:T(8,128)S(1)} %fusion.8, f32[768,6]{0,1:T(8,128)} %get-tuple-element.60, f32[6,64,64]{2,1,0:T(8,128)S(1)} %get-tuple-element.49, bf16[768,6,64]{0,2,1:T(8,128)(2,1)} %bitcast.116), kind=kOutput, calls=%fused_computation.38 | convolution fusion | flops 227667456 | bytes 3084288 | tf_op jit(solution)/shard_map/thd,hde->the/dot_general | solution.py:139
  72.1 1.6 %reshape.204 = f32[2,384,384]{1,0,2:T(2,128)} reshape(f32[768,6,64]{0,2,1:T(8,128)S(1)} %broadcast_multiply_fusion) | data formatting | bytes 2359296 | tf_op jit(solution)/shard_map/reshape | solution.py:144
  73.7 2.2 %fusion.35 = bf16[2,384,384]{1,2,0:T(8,128)(2,1)} fusion(f32[2,384,384]{1,0,2:T(2,128)} %reshape.204, f32[384]{0:T(512)S(1)} %copy-done.6), kind=kLoop, calls=%fused_computation.37 | loop fusion | flops 589824 | bytes 1771008 | tf_op jit(solution)/shard_map/convert_element_type | solution.py:144
  76.0 3.7 %all-to-all-start = ((bf16[2,384,384]{1,2,0:T(8,128)(2,1)}), bf16[2,384,384]{1,2,0:T(8,128)(2,1)S(1)}, u32[]{:S(2)}, u32[]{:S(2)}) async-start(bf16[2,384,384]{1,2,0:T(8,128)(2,1)} %fusion.35), calls=%async_computation | async-start | bytes 1179648 | tf_op jit(solution)/shard_map/all_to_all | solution.py:150
  79.7 4.6 %fusion.14 = bf16[768,384]{0,1:T(8,128)(2,1)} fusion(bf16[2048,384]{1,0:T(8,128)(2,1)} %param.20, bf16[1,768,2048]{2,1,0:T(8,128)(2,1)} %all-gather.6.cloned.1.call-done, f32[2048]{0:T(1024)S(1)} %copy-done.10, f32[768]{0:T(1024)S(1)} %add_rsqrt_fusion.1), kind=kOutput, calls=%fused_computation.29 | convolution fusion | flops 1213267968 | bytes 5319680 | tf_op jit(solution)/shard_map/dot_general | solution.py:94
  84.3 5.0 %fusion.62 = f32[384,2048]{1,0:T(8,128)} fusion(bf16[384,768]{0,1:T(8,128)(2,1)S(1)} %bitcast.112, bf16[768,2048]{1,0:T(8,128)(2,1)} %all-gather.8.cloned.1.call-done), kind=kOutput, calls=%fused_computation.79 | convolution fusion | flops 1207959552 | bytes 6881280 | tf_op jit(solution)/shard_map/dot_general | solution.py:153
  89.5 0.2 reshape.220
  89.7 1.0 copy.49
  90.6 1.8 %reshape.205 = bf16[6,128,2,3,64]{1,0,4,3,2:T(8,128)(2,1)S(1)} reshape(bf16[768,384]{0,1:T(8,128)(2,1)} %fusion.14) | data formatting | bytes 1179648 | tf_op jit(solution)/shard_map/reshape | solution.py:45
  92.4 1.0 copy.45
  93.4 0.8 pad_maximum_fusion
  94.3 0.4 copy.48
  94.7 0.8 pad_maximum_fusion.1
  95.7 1.0 copy.44
  96.7 1.8 %fusion.3 = (f32[2,3,6,128]{3,1,2,0:T(4,128)S(1)}, f32[2,6,256,128,3]{3,2,4,1,0:T(8,128)S(1)}) fusion(pred[6,128,256]{1,2,0:T(8,128)(4,1)S(1)} %broadcast_and_fusion, bf16[6,128,2,3,64]{1,0,4,3,2:T(8,128)(2,1)S(1)} %reshape.205, bf16[6,128,2,64]{1,3,0,2:T(8,128)(2,1)} %copy.49, bf16[6,128,2,64]{1,3,0,2:T(8,128)(2,1)S(1)} %copy.48), kind=kOutput, calls=%fused_computation.11 | convolution fusion | flops 155315712 | bytes 5916672 | tf_op jit(solution)/shard_map/nqhgd,nkhd->hgnqk/dot_general | solution.py:50
  98.6 1.1 fusion.2
  99.8 1.4 %fusion.26 = bf16[6,128,2,3,64]{1,4,3,2,0:T(8,128)(2,1)S(1)} fusion(bf16[6,128,2,64]{1,3,2,0:T(8,128)(2,1)S(1)} %copy-done.2, bf16[6,128,2,64]{1,3,2,0:T(8,128)(2,1)S(1)} %copy-done.3, f32[2,6,256,128,3]{3,2,4,1,0:T(8,128)S(1)} %get-tuple-element.65, f32[2,3,6,128]{3,1,2,0:T(4,128)S(1)} %exponential_add_fusion, ...), kind=kOutput, calls=%fused_computation.33 | convolution fusion | flops 157974528 | bytes 5935104 | tf_op jit(solution)/shard_map/hgnqk,nkhd->nqhgd/dot_general | solution.py:67
  101.2 0.4 copy.53
  101.6 0.4 convert_element_type.107
  102.1 0.9 copy.54
  103.0 3.5 %all-to-all-start.1 = ((bf16[2,384,384]{1,2,0:T(8,128)(2,1)}), bf16[2,384,384]{1,2,0:T(8,128)(2,1)S(1)}, u32[]{:S(2)}, u32[]{:S(2)}) async-start(bf16[2,384,384]{1,2,0:T(8,128)(2,1)} %copy.54), calls=%async_computation.1 | async-start | bytes 1179648 | tf_op jit(solution)/shard_map/all_to_all | solution.py:151
  106.5 1.7 %all-to-all-done.1 = bf16[2,384,384]{1,2,0:T(8,128)(2,1)S(1)} async-done(((bf16[2,384,384]{1,2,0:T(8,128)(2,1)}), bf16[2,384,384]{1,2,0:T(8,128)(2,1)S(1)}, u32[]{:S(2)}, u32[]{:S(2)}) %all-to-all-start.1) | async-done | bytes 589856 | tf_op jit(solution)/shard_map/all_to_all | solution.py:151
  108.2 5.4 %fusion.4 = bf16[1,384,2048]{2,1,0:T(8,128)(2,1)} fusion(f32[384,2048]{1,0:T(8,128)} %fusion.62, bf16[384,768]{0,1:T(8,128)(2,1)S(1)} %bitcast.113, bf16[768,2048]{1,0:T(8,128)(2,1)} %all-gather.10.cloned.1.call-done), kind=kOutput, calls=%fused_computation.13 | convolution fusion | flops 1209532416 | bytes 8454144 | tf_op jit(solution)/shard_map/dot_general | solution.py:157
  (63 shorter events, 2.0 us)
Async XLA Ops:
  6.5 33.2 %copy-start = (bf16[2048,384]{1,0:T(8,128)(2,1)S(1)}, bf16[2048,384]{1,0:T(8,128)(2,1)}, u32[]{:S(2)}) copy-start(bf16[2048,384]{1,0:T(8,128)(2,1)} %param.18) | copy-start | bytes 4718596
  6.5 7.0 %copy-start.14 = (u32[32]{0:T(128)S(1)}, u32[32]{0:T(128)}, u32[]{:S(2)}) copy-start(u32[32]{0:T(128)} %constant.59) | copy-start | bytes 388
  6.5 3.4 %copy-start.5 = (f32[1,6,768]{2,0,1:T(1,128)S(1)}, f32[1,6,768]{2,0,1:T(1,128)}, u32[]{:S(2)}) copy-start(f32[1,6,768]{2,0,1:T(1,128)} %param.23) | copy-start | bytes 55300
  6.5 8.5 %copy-start.11 = (f32[6]{0:T(128)S(1)}, f32[6]{0:T(128)}, u32[]{:S(2)}) copy-start(f32[6]{0:T(128)} %param.25) | copy-start | bytes 76
  6.5 22.4 %all-gather.6.cloned.1.call-start = ((), (), s32[]{:S(2)}) async-start(), calls=%async_computation.2 | async-start | bytes 4718592 | tf_op jit(solution)/shard_map/all_gather | solution.py:91
  7.3 77.0 %all-gather.8.cloned.1.call-start = ((), (), s32[]{:S(2)}) async-start(), calls=%async_computation.3 | async-start | bytes 4718592 | tf_op jit(solution)/shard_map/all_gather | solution.py:155
  8.0 23.7 %copy-start.8 = (bf16[2048,128]{1,0:T(8,128)(2,1)S(1)}, bf16[2048,128]{1,0:T(8,128)(2,1)}, u32[]{:S(2)}) copy-start(bf16[2048,128]{1,0:T(8,128)(2,1)} %param.21) | copy-start | bytes 1572868
  8.0 23.7 %copy-start.10 = (f32[2048]{0:T(1024)S(1)}, f32[2048]{0:T(1024)}, u32[]{:S(2)}) copy-start(f32[2048]{0:T(1024)} %param.16) | copy-start | bytes 24580
  8.0 98.4 %all-gather.10.cloned.1.call-start = ((), (), s32[]{:S(2)}) async-start(), calls=%async_computation.4 | async-start | bytes 4718592 | tf_op jit(solution)/shard_map/all_gather | solution.py:159
  12.1 0.6 copy-start.4
  28.9 2.8 %copy-start.1 = (bf16[1,768,2048]{2,1,0:T(8,128)(2,1)S(1)}, bf16[1,768,2048]{2,1,0:T(8,128)(2,1)}, u32[]{:S(2)}) copy-start(bf16[1,768,2048]{2,1,0:T(8,128)(2,1)} %all-gather.6.cloned.1.call-done) | copy-start | bytes 9437188
  31.8 3.5 %copy-start.9 = (bf16[2048,128]{1,0:T(8,128)(2,1)S(1)}, bf16[2048,128]{1,0:T(8,128)(2,1)}, u32[]{:S(2)}) copy-start(bf16[2048,128]{1,0:T(8,128)(2,1)} %param.22) | copy-start | bytes 1572868
  33.4 60.0 %collective-permute-start.1 = (bf16[128,128]{1,0:T(8,128)(2,1)}, bf16[128,128]{1,0:T(8,128)(2,1)}, u32[]{:S(2)}, u32[]{:S(2)}) collective-permute-start(bf16[128,128]{1,0:T(8,128)(2,1)} %slice.50), channel_id=1, source_target_pairs={{0,8},{8,16},{16,24},{1,9},{9,17},{17,25},{2,10},{10,18},{18,26},{... | collective-permute-start | bytes 98312 | tf_op jit(solution)/shard_map/ppermute | solution.py:36
  36.9 4.3 %copy-start.7 = (bf16[2048,384]{1,0:T(8,128)(2,1)S(1)}, bf16[2048,384]{1,0:T(8,128)(2,1)}, u32[]{:S(2)}) copy-start(bf16[2048,384]{1,0:T(8,128)(2,1)} %param.19) | copy-start | bytes 4718596
  36.9 57.9 %collective-permute-start = (bf16[128,128]{1,0:T(8,128)(2,1)}, bf16[128,128]{1,0:T(8,128)(2,1)}, u32[]{:S(2)}, u32[]{:S(2)}) collective-permute-start(bf16[128,128]{1,0:T(8,128)(2,1)} %slice.49), channel_id=1, source_target_pairs={{0,8},{8,16},{16,24},{1,9},{9,17},{17,25},{2,10},{10,18},{18,26},{... | collective-permute-start | bytes 98312 | tf_op jit(solution)/shard_map/ppermute | solution.py:36
  41.1 1.5 %copy-start.12 = (bf16[768,384]{0,1:T(8,128)(2,1)}, bf16[768,384]{0,1:T(8,128)(2,1)S(1)}, u32[]{:S(2)}) copy-start(bf16[768,384]{0,1:T(8,128)(2,1)S(1)} %fusion.13) | copy-start | bytes 1769476
  42.6 15.0 %copy-start.13 = (bf16[768,384]{0,1:T(8,128)(2,1)}, bf16[768,384]{0,1:T(8,128)(2,1)S(1)}, u32[]{:S(2)}) copy-start(bf16[768,384]{0,1:T(8,128)(2,1)S(1)} %fusion.11) | copy-start | bytes 1769476
  71.9 1.8 %copy-start.6 = (f32[384]{0:T(512)S(1)}, f32[384]{0:T(512)}, u32[]{:S(2)}) copy-start(f32[384]{0:T(512)} %param.24) | copy-start | bytes 4612
  76.0 8.3 %all-to-all-start = ((bf16[2,384,384]{1,2,0:T(8,128)(2,1)}), bf16[2,384,384]{1,2,0:T(8,128)(2,1)S(1)}, u32[]{:S(2)}, u32[]{:S(2)}) async-start(bf16[2,384,384]{1,2,0:T(8,128)(2,1)} %fusion.35), calls=%async_computation | async-start | bytes 1179648 | tf_op jit(solution)/shard_map/all_to_all | solution.py:150
  98.5 1.3 %copy-start.2 = (bf16[6,128,2,64]{1,3,2,0:T(8,128)(2,1)S(1)}, bf16[6,128,2,64]{1,3,2,0:T(8,128)(2,1)}, u32[]{:S(2)}) copy-start(bf16[6,128,2,64]{1,3,2,0:T(8,128)(2,1)} %copy.45) | copy-start | bytes 589828
  98.5 1.3 %copy-start.3 = (bf16[6,128,2,64]{1,3,2,0:T(8,128)(2,1)S(1)}, bf16[6,128,2,64]{1,3,2,0:T(8,128)(2,1)}, u32[]{:S(2)}) copy-start(bf16[6,128,2,64]{1,3,2,0:T(8,128)(2,1)} %copy.44) | copy-start | bytes 589828
  103.0 5.3 %all-to-all-start.1 = ((bf16[2,384,384]{1,2,0:T(8,128)(2,1)}), bf16[2,384,384]{1,2,0:T(8,128)(2,1)S(1)}, u32[]{:S(2)}, u32[]{:S(2)}) async-start(bf16[2,384,384]{1,2,0:T(8,128)(2,1)} %copy.54), calls=%async_computation.1 | async-start | bytes 1179648 | tf_op jit(solution)/shard_map/all_to_all | solution.py:151
Sparse Core Ops, SparseCore 0:
  8.9 14.8 all-gather.5
  25.3 13.2 all-gather.7
  40.2 13.2 all-gather.9
where the time goes:
time: 121 us; the launch traced here: 120 us
  matrix products  37.9 us (31%)
  blocking collectives  27.7 us (23%)
  between operations  14.1 us (12%)
  local copies, waits for them, and re-layouts  12.4 us (10%)
  starting transfers between devices  12 us (10%)
  other arithmetic  11.9 us (10%)
  waiting for transfers between devices  3.85 us (3%)
    all_gather x1, blocking collectives, prefix_2(): lax.all_gather(a.astype(kind), axis)  14.2 us
    dot_general x6, matrix products, shards(): jnp.dot(scaled, weight, preferred_element_type=jnp.float32)  14.1 us
    unnamed x1, blocking collectives  13.5 us
    dot_general x1, matrix products, shards(): jnp.einsum('hts,shd->thd', weights, shaped_v, preferred_element_type=jnp....  7.61 us
    dot_general x1, matrix products, shards(): jnp.dot(att_rows, lax.all_gather(out_att, 'tp', axis=0, tiled=True), pref...  5.42 us
    dot_general x1, matrix products, shards(): jnp.dot(ret_rows, lax.all_gather(retentive_exit_matrix, 'tp', axis=0, til...  5 us
    ppermute x2, starting transfers between devices, passed_along(): return lax.ppermute(value, axis, pairs)  4.7 us
    all_to_all x1, starting transfers between devices, shards(): lax.all_to_all(ret_out, 'tp', split_axis=0, concat_axis=1, tiled=True)  3.72 us
  transfers between devices with their start and end apart: 7, of which 1 were waited for; matrix products, arithmetic and copies ran while one was open for 47% of the time, Pallas kernels for 0%

commit v1 on v0

v1 whole, which is shorter than its diff:
```python
import functools

import jax
import jax.numpy as jnp
from jax import lax
from jax.experimental import pallas as pl
from jax.experimental.pallas import tpu as pltpu
from jax.sharding import PartitionSpec as P

HEAD_DIM = 64
WINDOW = 128
CHUNK = 128
LANES = 128
TILE = 256
EPS = 1e-06
F32 = jnp.float32
BF16 = jnp.bfloat16
EXACT = lax.Precision.HIGHEST

NT = (((1,), (1,)), ((), ()))
TN = (((0,), (0,)), ((), ()))


def layer(
    n_sp, n_tp, kv_heads,
    tok, gain, rq, rk, rv, aq, ak, av, ld, rgain, sink, wr, wa,
    out,
    xb, wb, acc, pb, inv, ldp, ct, cr, eq, ek, dm, st, ub, msg, inbox,
    hb, hin, wo, oacc,
    tok_sem, w_sem, wo_sem, x_send, x_recv, wo_send, wo_recv,
    h_send, h_recv, m_send, m_recv, halo_send, halo_recv,
):
    tp = lax.axis_index("tp")
    sp = lax.axis_index("sp")
    rows, depth = tok.shape
    ret_w, att_w, kv_w = rq.shape[1], aq.shape[1], ak.shape[1]
    heads = ld.shape[0]
    chunks = rows // CHUNK
    pairs = ret_w // LANES
    att_pairs = att_w // LANES
    att_heads = att_w // HEAD_DIM
    out_rows = rows // n_tp
    model = depth * n_tp
    scale = HEAD_DIM ** (-0.5)

    c_rk, c_rv, c_ak = 0, ret_w, 2 * ret_w
    c_av = c_ak + kv_w
    c_rq = c_av + kv_w
    c_aq = c_rq + ret_w
    width = c_aq + att_w
    parts = ((rk, c_rk), (rv, c_rv), (ak, c_ak), (av, c_av), (rq, c_rq), (aq, c_aq))
    kv_tiles, tiles = c_rq // TILE, width // TILE

    def load_tokens():
        return pltpu.make_async_copy(tok, xb.at[0], tok_sem)

    def load_weight(phase, i):
        owner = lax.rem(tp + phase, n_tp)
        ref, col = parts[i]
        return pltpu.make_async_copy(
            ref.at[pl.ds(owner * depth, depth), :],
            wb.at[phase, :, pl.ds(col, ref.shape[1])],
            w_sem.at[phase, i],
        )

    def load_exit(i):
        ref = (wr, wa)[i]
        return pltpu.make_async_copy(
            ref, wo.at[0, pl.ds(i * ret_w, ref.shape[0]), :], wo_sem.at[i]
        )

    def send_tokens(q):
        return pltpu.make_async_remote_copy(
            src_ref=tok, dst_ref=xb.at[n_tp - q],
            send_sem=x_send.at[q - 1], recv_sem=x_recv.at[n_tp - q - 1],
            device_id={"tp": lax.rem(tp + q, n_tp)}, device_id_type=pl.DeviceIdType.MESH,
        )

    def send_exit(q, i):
        ref = (wr, wa)[i]
        return pltpu.make_async_remote_copy(
            src_ref=ref, dst_ref=wo.at[n_tp - q, pl.ds(i * ret_w, ref.shape[0]), :],
            send_sem=wo_send.at[q - 1, i], recv_sem=wo_recv.at[n_tp - q - 1, i],
            device_id={"tp": lax.rem(tp + q, n_tp)}, device_id_type=pl.DeviceIdType.MESH,
        )

    def send_heads(q, i):
        target = lax.rem(tp + q, n_tp)
        cols = pl.ds(i * ret_w, (ret_w, att_w)[i])
        return pltpu.make_async_remote_copy(
            src_ref=hb.at[pl.ds(target * out_rows, out_rows), cols],
            dst_ref=hin.at[n_tp - q - 1, :, cols],
            send_sem=h_send.at[q - 1, i], recv_sem=h_recv.at[n_tp - q - 1, i],
            device_id={"tp": target}, device_id_type=pl.DeviceIdType.MESH,
        )

    def send_state(q):
        return pltpu.make_async_remote_copy(
            src_ref=msg, dst_ref=inbox.at[q - 1],
            send_sem=m_send.at[q - 1], recv_sem=m_recv.at[q - 1],
            device_id={"sp": lax.rem(sp + q, n_sp)}, device_id_type=pl.DeviceIdType.MESH,
        )

    def send_halo():
        cols = pl.ds(c_ak, 2 * kv_w)
        return pltpu.make_async_remote_copy(
            src_ref=pb.at[pl.ds(rows, WINDOW), cols],
            dst_ref=pb.at[pl.ds(0, WINDOW), cols],
            send_sem=halo_send, recv_sem=halo_recv,
            device_id={"sp": lax.rem(sp + 1, n_sp)}, device_id_type=pl.DeviceIdType.MESH,
        )

    barrier = pltpu.get_barrier_semaphore()
    for q in range(1, n_tp):
        pl.semaphore_signal(
            barrier, inc=1, device_id={"tp": lax.rem(tp + q, n_tp)},
            device_id_type=pl.DeviceIdType.MESH,
        )
    for q in range(1, n_sp):
        pl.semaphore_signal(
            barrier, inc=1, device_id={"sp": lax.rem(sp + q, n_sp)},
            device_id_type=pl.DeviceIdType.MESH,
        )
    load_tokens().start()
    for phase in range(n_tp):
        for i in range(len(parts)):
            load_weight(phase, i).start()

    lane = lax.broadcasted_iota(jnp.int32, (CHUNK, LANES), 1)
    row = lax.broadcasted_iota(jnp.int32, (CHUNK, LANES), 0)
    first_half = lane < HEAD_DIM
    lane1 = lax.broadcasted_iota(jnp.int32, (1, LANES), 1)
    half_masks = (
        jnp.where(lane1 < HEAD_DIM, 1.0, 0.0).astype(BF16),
        jnp.where(lane1 < HEAD_DIM, 0.0, 1.0).astype(BF16),
    )
    same_head = (row < HEAD_DIM) == first_half
    pad_rows = 8

    tri = jnp.where(lane <= row, 1.0, 0.0).astype(F32)
    ldp[...] = jnp.zeros_like(ldp)
    ldp[:heads, :] = ld[...]

    pl.semaphore_wait(barrier, n_tp - 1 + n_sp - 1)
    for q in range(1, n_tp):
        send_tokens(q).start()

    for c in range(chunks):
        span = slice(c * CHUNK, (c + 1) * CHUNK)
        part = ldp[:, span]
        ct[span, :] = lax.dot_general(
            tri, part, NT, precision=EXACT, preferred_element_type=F32
        )
        cr[c] = lax.dot_general(
            part[:pad_rows], tri, NT, precision=EXACT, preferred_element_type=F32
        )

    def decays(c, carry):
        span = pl.ds(pl.multiple_of(c * CHUNK, CHUNK), CHUNK)
        columns = ct[span, :]
        rows_c = cr[c]
        for p in range(pairs):
            wide = [
                jnp.broadcast_to(columns[:, h : h + 1], (CHUNK, LANES))
                for h in (2 * p, 2 * p + 1)
            ]
            mixed = jnp.where(first_half, wide[0], wide[1])
            cols = slice(p * LANES, (p + 1) * LANES)
            eq[span, cols] = jnp.exp(mixed)
            ek[span, cols] = jnp.exp(mixed[CHUNK - 1 :, :] - mixed) * scale
            for e in range(2):
                h = 2 * p + e
                gap = jnp.where(lane <= row, wide[e] - rows_c[h : h + 1, :], -jnp.inf)
                dm[c, h] = jnp.exp(gap) * scale
        return carry

    lax.fori_loop(0, chunks, decays, 0)

    def scaled(phase):
        owner = lax.rem(tp + phase, n_tp)
        factors = gain[owner]

        def one(i, carry):
            span = pl.ds(pl.multiple_of(i * CHUNK, CHUNK), CHUNK)
            x = xb[phase, span, :].astype(F32)
            xb[phase, span, :] = (x * factors).astype(BF16)
            squares = jnp.broadcast_to(
                jnp.sum(x * x, axis=1, keepdims=True), (CHUNK, LANES)
            )
            if phase > 0:
                squares = inv[span, :] + squares
            if phase == n_tp - 1:
                squares = lax.rsqrt(squares / model + EPS)
            inv[span, :] = squares
            return carry

        lax.fori_loop(0, chunks, one, 0)

    def project(phase, low, high):
        def one(n, carry):
            cols = pl.ds(pl.multiple_of(n * TILE, TILE), TILE)
            total = jnp.dot(xb[phase], wb[phase, :, cols], preferred_element_type=F32)
            if phase > 0:
                total = acc[:, cols] + total
            if phase == n_tp - 1:
                wide = jnp.concatenate([inv[...]] * (TILE // LANES), axis=1)
                pb[WINDOW:, cols] = (total * wide).astype(BF16)
            else:
                acc[:, cols] = total
            return carry

        lax.fori_loop(low, high, one, 0)

    load_tokens().wait()
    scaled(0)
    for i in range(4):
        load_weight(0, i).wait()
    project(0, 0, kv_tiles)
    for i in range(4, 6):
        load_weight(0, i).wait()
    for q in range(1, n_tp):
        for i in range(2):
            send_exit(q, i).start()
    for i in range(2):
        load_exit(i).start()
    project(0, kv_tiles, tiles)
    for phase in range(1, n_tp):
        for i in range(6):
            load_weight(phase, i).wait()
        send_tokens(n_tp - phase).wait_recv()
        scaled(phase)
        if phase < n_tp - 1:
            project(phase, 0, tiles)
    project(n_tp - 1, 0, kv_tiles)

    @pl.when(sp + 1 < n_sp)
    def _():
        send_halo().start()

    st[...] = jnp.zeros_like(st)

    def own_state(c, totals):
        span = pl.ds(pl.multiple_of(c * CHUNK, CHUNK), CHUNK)
        here = pl.ds(pl.multiple_of(WINDOW + c * CHUNK, CHUNK), CHUNK)
        after = []
        for p in range(pairs):
            cols = slice(p * LANES, (p + 1) * LANES)
            keys = pb[here, c_rk + p * LANES : c_rk + (p + 1) * LANES].astype(F32)
            values = pb[here, c_rv + p * LANES : c_rv + (p + 1) * LANES]
            keyed = (keys * ek[span, cols]).astype(BF16)
            added = lax.dot_general(keyed, values, TN, preferred_element_type=F32)
            added = jnp.where(same_head, added, 0.0)
            ub[c, p] = added
            fade = eq[span, cols][CHUNK - 1 :, :]
            st[p] = st[p] * fade + added
            after.append(totals[p] * fade)
        return tuple(after)

    totals = lax.fori_loop(
        0, chunks, own_state, tuple(jnp.ones((1, LANES), F32) for _ in range(pairs))
    )
    for p in range(pairs):
        msg[p, :HEAD_DIM, :] = (st[p, :HEAD_DIM, :] + st[p, HEAD_DIM:, :]).astype(BF16)
        coarse = totals[p].astype(BF16)
        fine = (totals[p] - coarse.astype(F32)).astype(BF16)
        row16 = lax.broadcasted_iota(jnp.int32, (16, LANES), 0)
        msg[p, HEAD_DIM:, :] = jnp.where(
            row16 == 0, coarse.astype(F32), jnp.where(row16 == 1, fine.astype(F32), 0.0)
        ).astype(BF16)

    for q in range(1, n_sp):
        @pl.when(sp + q < n_sp)
        def _():
            send_state(q).start()

    project(n_tp - 1, kv_tiles, tiles)

    blocks = rows // WINDOW
    q_at = lax.broadcasted_iota(jnp.int32, (WINDOW, 2 * WINDOW), 0)
    k_at = lax.broadcasted_iota(jnp.int32, (WINDOW, 2 * WINDOW), 1)
    distance = WINDOW + q_at - k_at
    in_window = (distance >= 0) & (distance < WINDOW)

    def attend(i, carry):
        n = blocks - 1 - i

        @pl.when((n == 0) & (sp > 0))
        def _():
            send_halo().wait_recv()

        @pl.when((n == 0) & (sp == 0))
        def _():
            pb[:WINDOW, c_ak : c_ak + 2 * kv_w] = jnp.zeros((WINDOW, 2 * kv_w), BF16)

        lowest = jnp.where((n == 0) & (sp == 0), WINDOW, 0)
        allowed = in_window & (k_at >= lowest)
        band = pl.ds(pl.multiple_of(n * WINDOW, WINDOW), 2 * WINDOW)
        here = pl.ds(pl.multiple_of((n + 1) * WINDOW, WINDOW), WINDOW)
        store = pl.ds(pl.multiple_of(n * WINDOW, WINDOW), WINDOW)
        kinds = {}
        for t in range(kv_w // LANES):
            for name, col in (("k", c_ak), ("v", c_av)):
                plain = pb[band, col + t * LANES : col + (t + 1) * LANES]
                turned = pltpu.roll(plain.astype(F32), HEAD_DIM, 1).astype(BF16)
                kinds[name, t] = (plain, turned)
        scores = []
        picks = []
        for h in range(att_heads):
            p, e = h // 2, h % 2
            g = h * kv_heads // att_heads
            picks.append((g // 2, int(g % 2 != e)))
            query = pb[here, c_aq + p * LANES : c_aq + (p + 1) * LANES] * half_masks[e]
            t, turn = picks[h]
            scores.append(
                lax.dot_general(query, kinds["k", t][turn], NT, preferred_element_type=F32)
            )
        weights = []
        for h in range(att_heads):
            s = jnp.where(allowed, scores[h] * scale, -jnp.inf)
            sink_h = sink[h]
            highest = jnp.maximum(jnp.max(s, axis=1, keepdims=True), sink_h)
            raised = jnp.exp(s - highest)
            total = jnp.sum(raised, axis=1, keepdims=True) + jnp.exp(sink_h - highest)
            weights.append((raised * (1.0 / total)).astype(BF16))
        for p in range(att_pairs):
            left = jnp.concatenate([weights[2 * p], weights[2 * p + 1]], axis=1)
            right = jnp.concatenate(
                [
                    kinds["v", picks[2 * p + e][0]][picks[2 * p + e][1]] * half_masks[e]
                    for e in range(2)
                ],
                axis=0,
            )
            hb[store, ret_w + p * LANES : ret_w + (p + 1) * LANES] = jnp.dot(
                left, right, preferred_element_type=F32
            ).astype(BF16)
        return carry

    lax.fori_loop(0, blocks, attend, 0)
    for q in range(1, n_tp):
        send_heads(q, 1).start()

    st[...] = jnp.zeros_like(st)
    for q in range(n_sp - 1, 0, -1):
        @pl.when(sp >= q)
        def _():
            send_state(q).wait_recv()
            for p in range(pairs):
                part = inbox[q - 1, p].astype(F32)
                fade = part[HEAD_DIM : HEAD_DIM + 1] + part[HEAD_DIM + 1 : HEAD_DIM + 2]
                both = jnp.concatenate([part[:HEAD_DIM]] * 2, axis=0)
                st[p] = st[p] * fade + jnp.where(same_head, both, 0.0)

    ones = jnp.where(same_head, 1.0, 0.0).astype(BF16)
    ones2 = jnp.concatenate([ones, ones], axis=0)

    def retain(c, carry):
        span = pl.ds(pl.multiple_of(c * CHUNK, CHUNK), CHUNK)
        here = pl.ds(pl.multiple_of(WINDOW + c * CHUNK, CHUNK), CHUNK)
        kept = []
        for p in range(pairs):
            cols = slice(p * LANES, (p + 1) * LANES)
            query = pb[here, c_rq + p * LANES : c_rq + (p + 1) * LANES]
            keys = pb[here, c_rk + p * LANES : c_rk + (p + 1) * LANES]
            values = pb[here, c_rv + p * LANES : c_rv + (p + 1) * LANES]
            left = [
                (
                    lax.dot_general(
                        query * half_masks[e], keys, NT, preferred_element_type=F32
                    )
                    * dm[c, 2 * p + e]
                ).astype(BF16)
                for e in range(2)
            ]
            state = st[p]
            faded = eq[span, cols]
            left.append((query.astype(F32) * faded).astype(BF16))
            right = [values * half_masks[0], values * half_masks[1], state.astype(BF16)]
            kept.append(
                jnp.dot(
                    jnp.concatenate(left, axis=1),
                    jnp.concatenate(right, axis=0),
                    preferred_element_type=F32,
                )
            )
            st[p] = state * faded[CHUNK - 1 :, :] + ub[c, p]
        for p in range(pairs):
            cols = slice(p * LANES, (p + 1) * LANES)
            r = kept[p]
            square = r * r
            coarse = square.astype(BF16)
            fine = (square - coarse.astype(F32)).astype(BF16)
            total = jnp.dot(
                jnp.concatenate([coarse, fine], axis=1), ones2, preferred_element_type=F32
            )
            normed = r * lax.rsqrt(total * (1.0 / HEAD_DIM) + EPS)
            hb[span, cols] = (normed * rgain[:, cols]).astype(BF16)
        return carry

    lax.fori_loop(0, chunks, retain, 0)
    for q in range(1, n_tp):
        send_heads(q, 0).start()

    for i in range(2):
        load_exit(i).wait()
    mine = pl.ds(pl.multiple_of(tp * out_rows, out_rows), out_rows)

    def leave(phase):
        def one(n, carry):
            cols = pl.ds(pl.multiple_of(n * TILE, TILE), TILE)
            left = hb[mine, :] if phase == 0 else hin[phase - 1]
            total = jnp.dot(left, wo[phase, :, cols], preferred_element_type=F32)
            if phase > 0:
                total = oacc[:, cols] + total
            if phase == n_tp - 1:
                out[:, cols] = total.astype(BF16)
            else:
                oacc[:, cols] = total
            return carry

        lax.fori_loop(0, model // TILE, one, 0)

    leave(0)
    for phase in range(1, n_tp):
        for i in range(2):
            send_exit(n_tp - phase, i).wait_recv()
            send_heads(n_tp - phase, i).wait_recv()
        leave(phase)

    for q in range(1, n_tp):
        send_tokens(q).wait_send()
        for i in range(2):
            send_exit(q, i).wait_send()
            send_heads(q, i).wait_send()
    for q in range(1, n_sp):
        @pl.when(sp + q < n_sp)
        def _():
            send_state(q).wait_send()

    @pl.when(sp + 1 < n_sp)
    def _():
        send_halo().wait_send()


def shards(n_sp, n_tp, tokens, in_gain, rq, rk, rv, aq, ak, av, log_decay, ret_gain, sink, wr, wa):
    rows, depth = tokens.shape[1:]
    ret_w, att_w, kv_w = rq.shape[1], aq.shape[1], ak.shape[1]
    heads = log_decay.shape[1]
    model = depth * n_tp
    width = 3 * ret_w + att_w + 2 * kv_w
    chunks, pairs = rows // CHUNK, ret_w // LANES
    out_rows = rows // n_tp
    kv_heads = kv_w // HEAD_DIM
    later = max(n_sp - 1, 1)
    others = max(n_tp - 1, 1)
    vmem = pl.BlockSpec(memory_space=pltpu.VMEM)
    hbm = pl.BlockSpec(memory_space=pltpu.HBM)
    smem = pl.BlockSpec(memory_space=pltpu.SMEM)
    dma = pltpu.SemaphoreType.DMA
    result = pl.pallas_call(
        functools.partial(layer, n_sp, n_tp, kv_heads),
        out_shape=jax.ShapeDtypeStruct((out_rows, model), BF16),
        in_specs=[hbm, vmem] + [hbm] * 6 + [vmem, vmem, smem, hbm, hbm],
        out_specs=vmem,
        scratch_shapes=[
            pltpu.VMEM((n_tp, rows, depth), BF16),
            pltpu.VMEM((n_tp, depth, width), BF16),
            pltpu.VMEM((rows, width), F32),
            pltpu.VMEM((WINDOW + rows, width), BF16),
            pltpu.VMEM((rows, LANES), F32),
            pltpu.VMEM((LANES, rows), F32),
            pltpu.VMEM((rows, LANES), F32),
            pltpu.VMEM((chunks, 8, CHUNK), F32),
            pltpu.VMEM((rows, ret_w), F32),
            pltpu.VMEM((rows, ret_w), F32),
            pltpu.VMEM((chunks, heads, CHUNK, CHUNK), F32),
            pltpu.VMEM((pairs, LANES, LANES), F32),
            pltpu.VMEM((chunks, pairs, LANES, LANES), F32),
            pltpu.VMEM((pairs, HEAD_DIM + 16, LANES), BF16),
            pltpu.VMEM((later, pairs, HEAD_DIM + 16, LANES), BF16),
            pltpu.VMEM((rows, ret_w + att_w), BF16),
            pltpu.VMEM((others, out_rows, ret_w + att_w), BF16),
            pltpu.VMEM((n_tp, ret_w + att_w, model), BF16),
            pltpu.VMEM((out_rows, model), F32),
            dma, dma((n_tp, 6)), dma((2,)),
            dma((others,)), dma((others,)),
            dma((others, 2)), dma((others, 2)),
            dma((others, 2)), dma((others, 2)),
            dma((later,)), dma((later,)),
            dma, dma,
        ],
        compiler_params=pltpu.CompilerParams(
            collective_id=0, has_side_effects=True, vmem_limit_bytes=60 * 1024 * 1024
        ),
    )(
        tokens[0], in_gain.reshape(n_tp, 1, depth), rq, rk, rv, aq, ak, av,
        log_decay[0], ret_gain.reshape(1, ret_w), sink, wr, wa,
    )
    return result[None]


def solution(mesh):
    n_sp, n_tp = mesh.shape["sp"], mesh.shape["tp"]
    return jax.shard_map(
        functools.partial(shards, n_sp, n_tp),
        mesh=mesh,
        in_specs=(
            P("fs", "sp", "tp"),
            P(),
            P(None, "tp"),
            P(None, "tp"),
            P(None, "tp"),
            P(None, "tp"),
            P(None, "tp"),
            P(None, "tp"),
            P("fs", "tp", "sp"),
            P("tp"),
            P("tp"),
            P("tp", None),
            P("tp", None),
        ),
        out_specs=P("fs", ("sp", "tp"), None),
        check_vma=False,
    )
```

time: 121 us -> 41.1 us (0.34)
  matrix products: 37.9 us -> 0 us
  Pallas kernels: 0 us -> 35.5 us
  blocking collectives: 27.7 us -> 0 us
  between operations: 14.1 us -> 0.01 us
  starting transfers between devices: 12 us -> 0 us
  other arithmetic: 11.9 us -> 0 us
  local copies, waits for them, and re-layouts: 12.4 us -> 5.31 us
  waiting for transfers between devices: 3.85 us -> 0 us
    dot_general x13 -> x0, matrix products: 37.9 us -> none  [the longest x6 14.1 us: shards(): jnp.dot(scaled, weight, preferred_element_type=jnp.float32)]
    pallas_call x0 -> x1, Pallas kernels: none -> 35.5 us  [shards(): pl.pallas_call(functools.partial(layer, n_sp, n_tp, kv_heads), out_shape=...]
    all_gather x1 -> x0, blocking collectives: 14.2 us -> none  [prefix_2(): lax.all_gather(a.astype(kind), axis)]
    unnamed x1 -> x0, blocking collectives: 13.5 us -> none
    all_to_all x2 -> x0, starting transfers between devices: 7.22 us -> none  [the longest x1 3.72 us: shards(): lax.all_to_all(ret_out, 'tp', split_axis=0, concat_axis=1, tiled=True)]
    slice x12 -> x0, local copies, waits for them, and re-layouts: 5.42 us -> none  [the longest x4 2.29 us: attend_window(): value_band = jnp.concatenate([value_blocks[:-1], value_blocks[1:]], axis=1)]
    ppermute x2 -> x0, starting transfers between devices: 4.7 us -> none  [passed_along(): return lax.ppermute(value, axis, pairs)]
    reduce_sum x2 -> x0, other arithmetic: 3.86 us -> none  [the longest x1 2.72 us: shards(): sums, squares = (sums, jnp.sum(wide * wide, axis=1, keepdims=True))]
  transfers between devices with their start and end apart: 7 -> 0, of which waited for: 1 -> 0; matrix products, arithmetic and copies ran while one was open for 47% -> 0% of each run, Pallas kernels for 0% -> 0%
where the time goes in v1:
time: 41.1 us; the launch traced here: 40.8 us
  Pallas kernels  35.5 us (86%)
  local copies, waits for them, and re-layouts  5.31 us (13%)
    pallas_call x1, Pallas kernels, shards(): pl.pallas_call(functools.partial(layer, n_sp, n_tp, kv_heads), out_shape=...  35.5 us
    unnamed x2, local copies, waits for them, and re-layouts  4.06 us
    reshape x1, local copies, waits for them, and re-layouts, shards(): ret_gain.reshape(1, ret_w)  1.25 us

profile of v1, /device:TPU:0, one launch (start us, length us, event | category | flops | bytes accessed | tf_op | source)
XLA Modules:
  0.0 40.8 jit_solution(2271360473859263934)
XLA Ops:
  0.0 1.3 %reshape.7.rgain = f32[1,384]{1,0:T(1,128)} reshape(f32[384]{0:T(512)} %param.22) | data formatting | bytes 3072 | tf_op jit(solution)/shard_map/reshape | solution.py:497
  1.3 1.3 %copy.16 = f32[1,6,768]{2,1,0:T(8,128)} copy(f32[1,6,768]{2,0,1:T(1,128)} %param.21) | data formatting | bytes 36864
  2.6 35.5 %shard_map.127 = bf16[384,2048]{1,0:T(8,128)(2,1)} custom-call(bf16[768,1024]{1,0:T(8,128)(2,1)} %bitcast.7, f32[2,1,1024]{2,1,0:T(1,128)} %bitcast.9, bf16[2048,384]{1,0:T(8,128)(2,1)} %rq.1, bf16[2048,384]{1,0:T(8,128)(2,1)} %rk.1, bf16[2048,384]{1,0:T(8,128)(2,1)} %rv.1, bf16[2048,384]{1,0:T(8,128)(2,1)} %aq.1, bf16[2048,128]{1,0:T(8,128)(2,1)} %ak.1, ...), custom_call_target="tpu_custom_call" | custom-call | tf_op jit(solution)/shard_map/pallas_call | solution.py:460
  38.1 2.7 %copy.18 = bf16[1,384,2048]{2,1,0:T(8,128)(2,1)} copy(bf16[1,384,2048]{2,1,0:T(8,128)(2,1)} %bitcast.6) | data formatting | bytes 3145728

commit v2 on v1

--- a/solution.py
+++ b/solution.py
@@ -12,6 +12,7 @@
 CHUNK = 128
 LANES = 128
 TILE = 256
+EXIT_TILE = 512
 EPS = 1e-06
 F32 = jnp.float32
 BF16 = jnp.bfloat16
@@ -23,18 +24,18 @@
 
 def layer(
     n_sp, n_tp, kv_heads,
-    tok, gain, rq, rk, rv, aq, ak, av, ld, rgain, sink, wr, wa,
+    tok, gain_in, rq, rk, rv, aq, ak, av, ld_in, rgain, sink, wr, wa,
     out,
     xb, wb, acc, pb, inv, ldp, ct, cr, eq, ek, dm, st, ub, msg, inbox,
     hb, hin, wo, oacc,
-    tok_sem, w_sem, wo_sem, x_send, x_recv, wo_send, wo_recv,
+    gain, ld, small_sem, tok_sem, w_sem, wo_sem, x_send, x_recv, wo_send, wo_recv,
     h_send, h_recv, m_send, m_recv, halo_send, halo_recv,
 ):
     tp = lax.axis_index("tp")
     sp = lax.axis_index("sp")
     rows, depth = tok.shape
     ret_w, att_w, kv_w = rq.shape[1], aq.shape[1], ak.shape[1]
-    heads = ld.shape[0]
+    heads = ld_in.shape[0]
     chunks = rows // CHUNK
     pairs = ret_w // LANES
     att_pairs = att_w // LANES
@@ -110,6 +111,10 @@
             device_id={"sp": lax.rem(sp + 1, n_sp)}, device_id_type=pl.DeviceIdType.MESH,
         )
 
+    rates = pltpu.make_async_copy(ld_in, ld, small_sem.at[0])
+    gains = pltpu.make_async_copy(gain_in, gain, small_sem.at[1])
+    rates.start()
+    gains.start()
     barrier = pltpu.get_barrier_semaphore()
     for q in range(1, n_tp):
         pl.semaphore_signal(
@@ -139,11 +144,9 @@
 
     tri = jnp.where(lane <= row, 1.0, 0.0).astype(F32)
     ldp[...] = jnp.zeros_like(ldp)
-    ldp[:heads, :] = ld[...]
-
-    pl.semaphore_wait(barrier, n_tp - 1 + n_sp - 1)
-    for q in range(1, n_tp):
-        send_tokens(q).start()
+    rates.wait()
+    for h in range(heads):
+        ldp[h : h + 1, :] = ld[h]
 
     for c in range(chunks):
         span = slice(c * CHUNK, (c + 1) * CHUNK)
@@ -176,6 +179,10 @@
 
     lax.fori_loop(0, chunks, decays, 0)
 
+    pl.semaphore_wait(barrier, n_tp - 1 + n_sp - 1)
+    for q in range(1, n_tp):
+        send_tokens(q).start()
+
     def scaled(phase):
         owner = lax.rem(tp + phase, n_tp)
         factors = gain[owner]
@@ -211,6 +218,7 @@
 
         lax.fori_loop(low, high, one, 0)
 
+    gains.wait()
     load_tokens().wait()
     scaled(0)
     for i in range(4):
@@ -257,7 +265,8 @@
         return tuple(after)
 
     totals = lax.fori_loop(
-        0, chunks, own_state, tuple(jnp.ones((1, LANES), F32) for _ in range(pairs))
+        0, chunks, own_state, tuple(jnp.ones((1, LANES), F32) for _ in range(pairs)),
+        unroll=2,
     )
     for p in range(pairs):
         msg[p, :HEAD_DIM, :] = (st[p, :HEAD_DIM, :] + st[p, HEAD_DIM:, :]).astype(BF16)
@@ -283,14 +292,6 @@
 
     def attend(i, carry):
         n = blocks - 1 - i
-
-        @pl.when((n == 0) & (sp > 0))
-        def _():
-            send_halo().wait_recv()
-
-        @pl.when((n == 0) & (sp == 0))
-        def _():
-            pb[:WINDOW, c_ak : c_ak + 2 * kv_w] = jnp.zeros((WINDOW, 2 * kv_w), BF16)
 
         lowest = jnp.where((n == 0) & (sp == 0), WINDOW, 0)
         allowed = in_window & (k_at >= lowest)
@@ -336,7 +337,17 @@
             ).astype(BF16)
         return carry
 
-    lax.fori_loop(0, blocks, attend, 0)
+    lax.fori_loop(0, blocks - 1, attend, 0)
+
+    @pl.when(sp > 0)
+    def _():
+        send_halo().wait_recv()
+
+    @pl.when(sp == 0)
+    def _():
+        pb[:WINDOW, c_ak : c_ak + 2 * kv_w] = jnp.zeros((WINDOW, 2 * kv_w), BF16)
+
+    lax.fori_loop(blocks - 1, blocks, attend, 0)
     for q in range(1, n_tp):
         send_heads(q, 1).start()
 
@@ -394,10 +405,10 @@
                 jnp.concatenate([coarse, fine], axis=1), ones2, preferred_element_type=F32
             )
             normed = r * lax.rsqrt(total * (1.0 / HEAD_DIM) + EPS)
-            hb[span, cols] = (normed * rgain[:, cols]).astype(BF16)
+            hb[span, cols] = (normed * rgain[cols].reshape(1, LANES)).astype(BF16)
         return carry
 
-    lax.fori_loop(0, chunks, retain, 0)
+    lax.fori_loop(0, chunks, retain, 0, unroll=2)
     for q in range(1, n_tp):
         send_heads(q, 0).start()
 
@@ -407,7 +418,7 @@
 
     def leave(phase):
         def one(n, carry):
-            cols = pl.ds(pl.multiple_of(n * TILE, TILE), TILE)
+            cols = pl.ds(pl.multiple_of(n * EXIT_TILE, EXIT_TILE), EXIT_TILE)
             left = hb[mine, :] if phase == 0 else hin[phase - 1]
             total = jnp.dot(left, wo[phase, :, cols], preferred_element_type=F32)
             if phase > 0:
@@ -418,7 +429,7 @@
                 oacc[:, cols] = total
             return carry
 
-        lax.fori_loop(0, model // TILE, one, 0)
+        lax.fori_loop(0, model // EXIT_TILE, one, 0)
 
     leave(0)
     for phase in range(1, n_tp):
@@ -459,8 +470,8 @@
     dma = pltpu.SemaphoreType.DMA
     result = pl.pallas_call(
         functools.partial(layer, n_sp, n_tp, kv_heads),
-        out_shape=jax.ShapeDtypeStruct((out_rows, model), BF16),
-        in_specs=[hbm, vmem] + [hbm] * 6 + [vmem, vmem, smem, hbm, hbm],
+        out_shape=pltpu.VMEM((out_rows, model), BF16),
+        in_specs=[hbm] * 9 + [vmem, smem, hbm, hbm],
         out_specs=vmem,
         scratch_shapes=[
             pltpu.VMEM((n_tp, rows, depth), BF16),
@@ -482,6 +493,9 @@
             pltpu.VMEM((others, out_rows, ret_w + att_w), BF16),
             pltpu.VMEM((n_tp, ret_w + att_w, model), BF16),
             pltpu.VMEM((out_rows, model), F32),
+            pltpu.VMEM((n_tp, 1, depth), F32),
+            pltpu.VMEM((heads, 1, rows), F32),
+            dma((2,)),
             dma, dma((n_tp, 6)), dma((2,)),
             dma((others,)), dma((others,)),
             dma((others, 2)), dma((others, 2)),
@@ -490,11 +504,11 @@
             dma, dma,
         ],
         compiler_params=pltpu.CompilerParams(
-            collective_id=0, has_side_effects=True, vmem_limit_bytes=60 * 1024 * 1024
+            collective_id=0, has_side_effects=True, vmem_limit_bytes=52 * 1024 * 1024
         ),
     )(
         tokens[0], in_gain.reshape(n_tp, 1, depth), rq, rk, rv, aq, ak, av,
-        log_decay[0], ret_gain.reshape(1, ret_w), sink, wr, wa,
+        jnp.transpose(log_decay, (1, 0, 2)), ret_gain, sink, wr, wa,
     )
     return result[None]
 

time: 41.1 us -> 33.3 us (0.81)
  Pallas kernels: 35.5 us -> 29.1 us
  local copies, waits for them, and re-layouts: 5.31 us -> 3.9 us
    pallas_call x1, Pallas kernels: 35.5 us -> 29.1 us  [shards(): pl.pallas_call(functools.partial(layer, n_sp, n_tp, kv_heads), out_shape=...]
    reshape x1 -> x0, local copies, waits for them, and re-layouts: 1.25 us -> none  [shards(): ret_gain.reshape(1, ret_w)]
    unnamed x2 -> x9, local copies, waits for them, and re-layouts: 4.06 us -> 3.9 us
where the time goes in v2:
time: 33.3 us; the launch traced here: 33 us
  Pallas kernels  29.1 us (87%)
  local copies, waits for them, and re-layouts  3.9 us (12%)
    pallas_call x1, Pallas kernels, shards(): pl.pallas_call(functools.partial(layer, n_sp, n_tp, kv_heads), out_shape=...  29.1 us
    unnamed x9, local copies, waits for them, and re-layouts  3.9 us

profile of v2, /device:TPU:0, one launch (start us, length us, event | category | flops | bytes accessed | tf_op | source)
XLA Modules:
  0.0 33.0 jit_solution(16854446406742585682)
XLA Ops:
  0.0 0.0 copy-start
  0.0 0.7 %copy-done = f32[1,6,768]{2,0,1:T(1,128)S(1)} copy-done((f32[1,6,768]{2,0,1:T(1,128)S(1)}, f32[1,6,768]{2,0,1:T(1,128)}, u32[]{:S(2)}) %copy-start) | copy-done | bytes 18456
  0.7 0.0 copy-start.1
  0.7 0.7 %copy-done.1 = f32[2048]{0:T(1024)S(1)} copy-done((f32[2048]{0:T(1024)S(1)}, f32[2048]{0:T(1024)}, u32[]{:S(2)}) %copy-start.1) | copy-done | bytes 8216
  1.4 0.0 copy-start.2
  1.4 0.7 %copy-done.2 = f32[384]{0:T(512)S(1)} copy-done((f32[384]{0:T(512)S(1)}, f32[384]{0:T(512)}, u32[]{:S(2)}) %copy-start.2) | copy-done | bytes 1560
  2.1 0.0 copy-start.3
  2.1 0.7 %copy-done.3 = f32[6]{0:T(128)S(1)} copy-done((f32[6]{0:T(128)S(1)}, f32[6]{0:T(128)}, u32[]{:S(2)}) %copy-start.3) | copy-done | bytes 48
  2.8 29.1 %shard_map.127 = bf16[384,2048]{1,0:T(8,128)(2,1)S(1)} custom-call(bf16[768,1024]{1,0:T(8,128)(2,1)} %bitcast.7, f32[2,1,1024]{2,1,0:T(1,128)S(1)} %bitcast.6, bf16[2048,384]{1,0:T(8,128)(2,1)} %rq.1, bf16[2048,384]{1,0:T(8,128)(2,1)} %rk.1, bf16[2048,384]{1,0:T(8,128)(2,1)} %rv.1, bf16[2048,384]{1,0:T(8,128)(2,1)} %aq.1, bf16[2048,128]{1,0:T(8,128)(2,1)} %ak.1, ...), custom_call_target="tpu_custom_call" | custom-call | tf_op jit(solution)/shard_map/pallas_call | solution.py:471
  31.9 1.1 %copy.15 = bf16[1,384,2048]{2,1,0:T(8,128)(2,1)} copy(bf16[1,384,2048]{2,1,0:T(8,128)(2,1)S(1)} %bitcast.4) | data formatting | bytes 3145728
Async XLA Ops:
  0.0 0.7 %copy-start = (f32[1,6,768]{2,0,1:T(1,128)S(1)}, f32[1,6,768]{2,0,1:T(1,128)}, u32[]{:S(2)}) copy-start(f32[1,6,768]{2,0,1:T(1,128)} %param.21) | copy-start | bytes 55300
  0.7 0.7 %copy-start.1 = (f32[2048]{0:T(1024)S(1)}, f32[2048]{0:T(1024)}, u32[]{:S(2)}) copy-start(f32[2048]{0:T(1024)} %param.14) | copy-start | bytes 24580
  1.4 0.7 %copy-start.2 = (f32[384]{0:T(512)S(1)}, f32[384]{0:T(512)}, u32[]{:S(2)}) copy-start(f32[384]{0:T(512)} %rgain.1) | copy-start | bytes 4612
  2.1 0.7 %copy-start.3 = (f32[6]{0:T(128)S(1)}, f32[6]{0:T(128)}, u32[]{:S(2)}) copy-start(f32[6]{0:T(128)} %sink.1) | copy-start | bytes 76
